TPU v7x, 32 devices: a whole 2x2x4 slice. The times are simulated.
32 devices in a mesh: sp: 16 (over z, y, x), dp: 2 (over core).
Axes of the slice: x: 2, y: 2, z: 4, core: 2. Of those that a mesh axis runs over, the one named last changes fastest.
Arguments:
- tokens: bfloat16 [2048, 2048], P('sp', 'dp'), may hold values from -6 to 6
- cotangent: bfloat16 [2048, 2048], P('sp', 'dp'), may hold values from -6 to 6
- in_weight: bfloat16 [256, 2048], P('sp', 'dp'), may hold values from -0.125 to 0.125
- out_weight: bfloat16 [256, 2048], P('sp', 'dp'), may hold values from -0.375 to 0.375
- decay_rate: float32 [16, 32], P('sp'), may hold values from 0 to 1
- frequency: float32 [16, 32], P('sp'), may hold values from 4 to 40
- step_log: float32 [16], P('sp'), may hold values from -2.6593 to -1.9661
- drive_real: float32 [16, 32, 16], P('sp'), may hold values from -6 to 6
- drive_imag: float32 [16, 32, 16], P('sp'), may hold values from -6 to 6
- readout_real_part: float32 [16, 16, 32], P('sp'), may hold values from -0.75 to 0.75
- readout_imaginary: float32 [16, 16, 32], P('sp'), may hold values from -0.75 to 0.75
- skip_gain: float32 [16, 16], P('sp'), may hold values from -4 to 4
Outputs:
- grad_tokens: bfloat16 [2048, 2048], P('sp', 'dp')
- grad_in_weight: float32 [256, 2048], P('sp', 'dp')
- grad_out_weight: float32 [256, 2048], P('sp', 'dp')
All inputs are finite; a program needn't handle non-finite values.
Results may differ from a plain program's by a relative error of at most 0.02.
Values may be sent and summed in bfloat16 or wider, within the bound.
A program may use at most 64 MiB of HBM per device.

v0:
```python
import jax
import jax.numpy as jnp
from jax import lax
from jax.sharding import PartitionSpec as P

finest_precision = lax.Precision.HIGHEST


def combine(earlier, later):
    first_real, first_imag, first_sum_real, first_sum_imag = earlier
    next_real, next_imag, next_sum_real, next_sum_imag = later
    return (
        first_real * next_real - first_imag * next_imag,
        first_real * next_imag + first_imag * next_real,
        next_real * first_sum_real - next_imag * first_sum_imag + next_sum_real,
        next_real * first_sum_imag + next_imag * first_sum_real + next_sum_imag,
    )


def discretize(decay_rate, frequency, step_log, drive_real, drive_imag):
    step_size = jnp.exp(step_log)[..., None]
    magnitude = jnp.exp(-decay_rate * step_size)
    angle = frequency * step_size
    decay_real = magnitude * jnp.cos(angle)
    decay_imag = magnitude * jnp.sin(angle)
    modulus = decay_rate * decay_rate + frequency * frequency
    hold_real = (-decay_rate * (decay_real - 1.0) + frequency * decay_imag) / modulus
    hold_imag = (-frequency * (decay_real - 1.0) - decay_rate * decay_imag) / modulus
    input_real = hold_real[..., None] * drive_real - hold_imag[..., None] * drive_imag
    input_imag = hold_real[..., None] * drive_imag + hold_imag[..., None] * drive_real
    return (decay_real, decay_imag, input_real, input_imag)


def mechanism(head_drive, head_back, params):
    (
        decay_rate,
        frequency,
        step_log,
        drive_real,
        drive_imag,
        readout_real_part,
        readout_imaginary,
        skip_gain,
    ) = params
    group_count, states = decay_rate.shape
    own_width, length = head_drive.shape
    per_group = own_width // group_count
    block_len = min(512, length)
    blocks_total = length // block_len
    decay_real, decay_imag, input_real, input_imag = discretize(
        decay_rate, frequency, step_log, drive_real, drive_imag
    )
    factor_real = jnp.broadcast_to(decay_real[:, :, None], (group_count, states, block_len))
    factor_imag = jnp.broadcast_to(decay_imag[:, :, None], (group_count, states, block_len))

    def to_blocks(matrix):
        shaped = matrix.astype(jnp.float32).reshape(group_count, per_group, blocks_total, block_len)
        return jnp.moveaxis(shaped, 2, 0)

    def forward(carried, drive_block):
        state_real, state_imag = carried
        push_real = jnp.einsum("gpc,gck->gpk", input_real, drive_block, precision=finest_precision)
        push_imag = jnp.einsum("gpc,gck->gpk", input_imag, drive_block, precision=finest_precision)
        push_real = push_real.at[:, :, 0].add(decay_real * state_real - decay_imag * state_imag)
        push_imag = push_imag.at[:, :, 0].add(decay_real * state_imag + decay_imag * state_real)
        _, _, running_real_part, running_imaginary = lax.associative_scan(
            combine, (factor_real, factor_imag, push_real, push_imag), axis=2
        )
        mixed_rows = (
            jnp.einsum(
                "mow,mwn->mon", readout_real_part, running_real_part, precision=finest_precision
            )
            - jnp.einsum(
                "mow,mwn->mon", readout_imaginary, running_imaginary, precision=finest_precision
            )
            + skip_gain[:, :, None] * drive_block
        )
        return ((running_real_part[:, :, -1], running_imaginary[:, :, -1]), mixed_rows)

    empty_state = jnp.zeros((group_count, states), jnp.float32)
    _, mixed_blocks = lax.scan(forward, (empty_state, empty_state), to_blocks(head_drive))

    def backward(carried, inputs):
        adjoint_real, adjoint_imag = carried
        mixed_rows, back_block = inputs
        gated, pullback = jax.vjp(jax.nn.gelu, mixed_rows)
        (interior_gradient,) = pullback(back_block)
        pulled_real_part = jnp.einsum(
            "woy,wom->wym", readout_real_part, interior_gradient, precision=finest_precision
        )[:, :, ::-1]
        pulled_imaginary = -jnp.einsum(
            "woy,wom->wym", readout_imaginary, interior_gradient, precision=finest_precision
        )[:, :, ::-1]
        pulled_real_part = pulled_real_part.at[:, :, 0].add(
            decay_real * adjoint_real + decay_imag * adjoint_imag
        )
        pulled_imaginary = pulled_imaginary.at[:, :, 0].add(
            decay_real * adjoint_imag - decay_imag * adjoint_real
        )
        _, _, running_real_part, running_imaginary = lax.associative_scan(
            combine, (factor_real, -factor_imag, pulled_real_part, pulled_imaginary), axis=2
        )
        running_real_part = running_real_part[:, :, ::-1]
        running_imaginary = running_imaginary[:, :, ::-1]
        grad_block = (
            jnp.einsum("gpc,gpk->gck", input_real, running_real_part, precision=finest_precision)
            + jnp.einsum("gpc,gpk->gck", input_imag, running_imaginary, precision=finest_precision)
            + skip_gain[:, :, None] * interior_gradient
        )
        return (
            (running_real_part[:, :, 0], running_imaginary[:, :, 0]),
            (grad_block.astype(jnp.bfloat16), gated.astype(jnp.bfloat16)),
        )

    _, (grad_blocks, gated_blocks) = lax.scan(
        backward, (empty_state, empty_state), (mixed_blocks, to_blocks(head_back)), reverse=True
    )

    def from_blocks(stacked):
        return jnp.moveaxis(stacked, 0, 2).reshape(own_width, length)

    return (from_blocks(grad_blocks), from_blocks(gated_blocks))


def on_device(
    tokens,
    cotangent,
    in_weight,
    out_weight,
    decay_rate,
    frequency,
    step_log,
    drive_real,
    drive_imag,
    readout_real_part,
    readout_imaginary,
    skip_gain,
):
    full_in, full_out = (
        lax.all_gather(in_weight, "sp", axis=0, tiled=True),
        lax.all_gather(out_weight, "sp", axis=0, tiled=True),
    )
    part_drive = jnp.einsum(
        "cd,td->ct", full_in, tokens, preferred_element_type=jnp.float32
    ).astype(jnp.bfloat16)
    part_back = jnp.einsum(
        "cd,td->ct", full_out, cotangent, preferred_element_type=jnp.float32
    ).astype(jnp.bfloat16)
    channels = part_drive.shape[0]
    rows_here = tokens.shape[0]
    seq_devices = lax.axis_size("sp")
    own_width = channels // seq_devices
    params = (
        decay_rate,
        frequency,
        step_log,
        drive_real,
        drive_imag,
        readout_real_part,
        readout_imaginary,
        skip_gain,
    )
    row_groups = lax.axis_size("dp")
    portion = rows_here // row_groups
    own_slot = lax.axis_index("dp") * portion
    drive_share, back_share = (
        lax.psum_scatter(part_drive, "dp", scatter_dimension=1, tiled=True).astype(jnp.float32),
        lax.psum_scatter(part_back, "dp", scatter_dimension=1, tiled=True).astype(jnp.float32),
    )
    drive_slice = drive_share.astype(jnp.bfloat16)[:, None, :]
    back_slice = back_share.astype(jnp.bfloat16)[:, None, :]
    drive_parts, back_parts = (
        lax.all_to_all(drive_slice, "sp", split_axis=0, concat_axis=1, tiled=True),
        lax.all_to_all(back_slice, "sp", split_axis=0, concat_axis=1, tiled=True),
    )
    drive_joined, back_joined = (
        lax.all_gather(drive_parts, "dp", axis=2, tiled=True),
        lax.all_gather(back_parts, "dp", axis=2, tiled=True),
    )
    head_grad, head_gated = mechanism(
        drive_joined.reshape(own_width, seq_devices * rows_here),
        back_joined.reshape(own_width, seq_devices * rows_here),
        params,
    )
    grad_slice = lax.dynamic_slice_in_dim(
        head_grad.reshape(own_width, seq_devices, rows_here), own_slot, portion, 2
    )
    gated_slice = lax.dynamic_slice_in_dim(
        head_gated.reshape(own_width, seq_devices, rows_here), own_slot, portion, 2
    )
    grad_parts, gated_parts = (
        lax.all_to_all(grad_slice, "sp", split_axis=1, concat_axis=0, tiled=True),
        lax.all_to_all(gated_slice, "sp", split_axis=1, concat_axis=0, tiled=True),
    )
    grad_joined, gated_joined = (
        lax.all_gather(grad_parts, "dp", axis=2, tiled=True),
        lax.all_gather(gated_parts, "dp", axis=2, tiled=True),
    )
    grad_cols = grad_joined.reshape(channels, rows_here)
    gated_cols = gated_joined.reshape(channels, rows_here)
    grad_tokens = jnp.einsum(
        "ct,cd->td", grad_cols, full_in, preferred_element_type=jnp.float32
    ).astype(jnp.bfloat16)
    grad_scale = (rows_here * seq_devices) ** (-0.5)
    picked = grad_cols
    grad_in_weight = lax.psum_scatter(
        jnp.einsum("ct,td->cd", picked, tokens, preferred_element_type=jnp.float32) * grad_scale,
        "sp",
        scatter_dimension=0,
        tiled=True,
    )
    picked = gated_cols
    grad_out_weight = lax.psum_scatter(
        jnp.einsum("ct,td->cd", picked, cotangent, preferred_element_type=jnp.float32) * grad_scale,
        "sp",
        scatter_dimension=0,
        tiled=True,
    )
    return (grad_tokens, grad_in_weight, grad_out_weight)


def solution(mesh):
    return jax.shard_map(
        on_device,
        mesh=mesh,
        in_specs=(
            P("sp", "dp"),
            P("sp", "dp"),
            P("sp", "dp"),
            P("sp", "dp"),
            P("sp", None),
            P("sp", None),
            P("sp"),
            P("sp", None, None),
            P("sp", None, None),
            P("sp", None, None),
            P("sp", None, None),
            P("sp", None),
        ),
        out_specs=(P("sp", "dp"), P("sp", "dp"), P("sp", "dp")),
        check_vma=False,
    )
```

profile of v0, /device:TPU:0, one launch (start us, length us, event | category | flops | bytes accessed | tf_op | source)
XLA Modules:
  0.0 653.4 jit_solution(1180258322243700626)
XLA Ops:
  7.2 45.7 %all_gather.20 = bf16[256,1024]{1,0:T(8,128)(2,1)S(1)} all-gather(bf16[16,1024]{1,0:T(8,128)(2,1)} %param.26), channel_id=1, replica_groups=mesh['sp'=16,'dp'=2] {'sp'}, dimensions={0}, use_global_device_ids=true | all-gather | bytes 557056 | tf_op jit(solution)/shard_map/all_gather | solution.py:140
  54.6 38.5 %all_gather.18 = bf16[256,1024]{1,0:T(8,128)(2,1)S(1)} all-gather(bf16[16,1024]{1,0:T(8,128)(2,1)S(1)} %copy-done.4), channel_id=1, replica_groups=mesh['sp'=16,'dp'=2] {'sp'}, dimensions={0}, use_global_device_ids=true | all-gather | bytes 557056 | tf_op jit(solution)/shard_map/all_gather | solution.py:141
  96.9 1.4 reduce.23
  99.1 3.5 all-to-all-start.1
  103.0 1.4 reduce.22
  105.2 4.8 all-to-all-done.1
  110.0 3.5 all-to-all-start
  114.0 2.2 all-gather.1
  118.6 164.4 %while.40 = (s32[]{:T(128)}, f32[1,32]{1,0:T(1,128)S(1)}, f32[1,32]{1,0:T(1,128)S(1)}, f32[4,1,16,512]{3,2,1,0:T(8,128)S(1)}, f32[4,1,16,512]{3,0,2,1:T(4,128)S(...) while((s32[]{:T(128)}, f32[1,32]{1,0:T(1,128)S(1)}, ...), condition=%wide.region_2.3_spmd, body=%wide.region_1.0_spmd.sunk | while | flops 12997378 | bytes 4572589 | solution.py:81
  120.7 1.1 slice.2926
  123.1 1.1 slice.2925
  124.2 1.1 slice.2922
  125.4 1.1 slice.2924
  152.1 1.1 slice.2995
  153.2 1.1 slice.2996
  161.7 1.1 slice.2926
  164.1 1.1 slice.2925
  165.3 1.1 slice.2922
  166.4 1.1 slice.2924
  193.2 1.1 slice.2995
  194.3 1.1 slice.2996
  202.8 1.1 slice.2926
  205.2 1.1 slice.2925
  206.3 1.1 slice.2922
  207.5 1.1 slice.2924
  234.2 1.1 slice.2995
  235.4 1.1 slice.2996
  243.8 1.1 slice.2926
  246.3 1.1 slice.2925
  247.4 1.1 slice.2922
  248.5 1.1 slice.2924
  274.1 1.1 slice.2994
  276.4 1.1 slice.2996
  283.4 2.2 all-gather
  287.3 188.4 %while.41 = (s32[]{:T(128)}, f32[1,32]{1,0:T(1,128)S(1)}, f32[1,32]{1,0:T(1,128)S(1)}, bf16[4,1,16,512]{3,2,1,0:T(8,128)(2,1)S(1)}, bf16[4,1,16,512]{3,2,1,0:T(8...) while((s32[]{:T(128)}, f32[1,32]{1,0:T(1,128)S(1)}, ...), condition=%wide.region_5.6_spmd, body=%wide.region_4.0_spmd.sunk | while | flops 13562627 | bytes 5699549 | solution.py:115
  307.7 1.1 slice.3051
  310.2 1.1 slice.3050
  311.3 1.1 slice.3047
  312.5 1.1 slice.3049
  339.2 1.1 slice.3120
  344.3 1.1 pad.1013
  350.4 1.1 slice.3051
  352.8 1.1 slice.3050
  354.0 1.1 slice.3047
  355.1 1.1 slice.3049
  387.0 1.1 pad.1013
  393.1 1.1 slice.3051
  395.5 1.1 slice.3050
  396.7 1.1 slice.3047
  397.8 1.1 slice.3049
  429.6 1.1 pad.1013
  435.7 1.1 slice.3051
  438.2 1.1 slice.3050
  439.3 1.1 slice.3047
  440.5 1.1 slice.3049
  472.3 1.1 pad.1013
  476.2 14.1 %all_to_all.72 = bf16[16,2,512]{2,1,0:T(2,128)(2,1)S(1)} all-to-all(bf16[16,2,512]{2,1,0:T(2,128)(2,1)S(1)} %reshape.604), channel_id=1, replica_groups=mesh['sp'=16,'dp'=2] {'sp'}, dimensions={0} | all-to-all | bytes 65536 | tf_op jit(solution)/shard_map/all_to_all | solution.py:193
  490.4 1.9 all_gather.23
  492.3 1.3 convolution_multiply_fusion
  493.8 10.1 %all_to_all.73 = bf16[16,2,512]{2,1,0:T(2,128)(2,1)S(1)} all-to-all(bf16[16,2,512]{2,1,0:T(2,128)(2,1)S(1)} %reshape.602), channel_id=1, replica_groups=mesh['sp'=16,'dp'=2] {'sp'}, dimensions={0} | all-to-all | bytes 65536 | tf_op jit(solution)/shard_map/all_to_all | solution.py:192
  504.1 1.9 all_gather.22
  506.0 1.3 convolution_multiply_fusion.1
  508.2 60.7 %reduce-scatter.11.cloned.1.call-done = f32[16,1024]{1,0:T(8,128)} async-done(((f32[256,1024]{1,0:T(8,128)}), f32[16,1024]{1,0:T(8,128)}) %reduce-scatter.11.cloned.1.call-update) | async-done | bytes 65552 | tf_op jit(solution)/shard_map/reduce_scatter | solution.py:213
  568.9 77.7 %reduce-scatter.9.cloned.1.call-done = f32[16,1024]{1,0:T(8,128)} async-done(((f32[256,1024]{1,0:T(8,128)}), f32[16,1024]{1,0:T(8,128)}) %reduce-scatter.9.cloned.1.call-update) | async-done | bytes 65552 | tf_op jit(solution)/shard_map/reduce_scatter | solution.py:206
  (1468 shorter events, 289.6 us)
Async XLA Ops:
  7.2 86.0 %copy-start = (bf16[128,1024]{1,0:T(8,128)(2,1)S(1)}, bf16[128,1024]{1,0:T(8,128)(2,1)}, u32[]{:S(2)}) copy-start(bf16[128,1024]{1,0:T(8,128)(2,1)} %param.25) | copy-start | bytes 786436
  7.2 45.7 %copy-start.1 = (bf16[128,1024]{1,0:T(8,128)(2,1)S(1)}, bf16[128,1024]{1,0:T(8,128)(2,1)}, u32[]{:S(2)}) copy-start(bf16[128,1024]{1,0:T(8,128)(2,1)} %param.24) | copy-start | bytes 786436
  7.2 89.1 %reduce-scatter.7.cloned.1.call-start = ((), (), s32[]{:S(2)}) async-start(), calls=%async_computation.9 | async-start | bytes 98304 | tf_op jit(solution)/shard_map/reduce_scatter | solution.py:167
  53.9 0.8 copy-start.4
  53.9 49.1 %reduce-scatter.5.cloned.1.call-start = ((), (), s32[]{:S(2)}) async-start(), calls=%async_computation.8 | async-start | bytes 98304 | tf_op jit(solution)/shard_map/reduce_scatter | solution.py:168
  94.8 0.7 copy-start.8
  94.9 0.7 copy-start.9
  95.6 0.7 copy-start.6
  95.6 0.7 copy-start.7
  99.1 10.9 %all-to-all-start.1 = ((bf16[16,2,512]{2,1,0:T(2,128)(2,1)}), bf16[16,2,512]{2,1,0:T(2,128)(2,1)S(1)}, u32[]{:S(2)}, u32[]{:S(2)}) async-start(bf16[16,2,512]{2,1,0:T(2,128)(2,1)} %reshape.600), calls=%async_computation.3 | async-start | bytes 65536 | tf_op jit(solution)/shard_map/all_to_all | solution.py:173
  110.0 173.0 %all-to-all-start = ((bf16[16,2,512]{2,1,0:T(2,128)(2,1)}), bf16[16,2,512]{2,1,0:T(2,128)(2,1)S(1)}, u32[]{:S(2)}, u32[]{:S(2)}) async-start(bf16[16,2,512]{2,1,0:T(2,128)(2,1)} %reshape.598), calls=%async_computation.1 | async-start | bytes 65536 | tf_op jit(solution)/shard_map/all_to_all | solution.py:174
  113.5 455.4 %reduce-scatter.11.cloned.1.call-start = ((), (), s32[]{:S(2)}) async-start(), calls=%async_computation.11 | async-start | bytes 1114112 | tf_op jit(solution)/shard_map/reduce_scatter | solution.py:213
  117.8 0.7 copy-start.2
  117.8 0.7 copy-start.3
  117.9 0.7 copy-start.5
  493.6 153.0 %reduce-scatter.9.cloned.1.call-start = ((), (), s32[]{:S(2)}) async-start(), calls=%async_computation.10 | async-start | bytes 1114112 | tf_op jit(solution)/shard_map/reduce_scatter | solution.py:206
Sparse Core Ops, SparseCore 0:
  54.0 3.3 reduce-scatter.6
  94.3 5.1 reduce-scatter.4
  493.7 75.1 reduce-scatter.10
  571.6 75.0 reduce-scatter.8
where the time goes:
time: 657 us; the launch traced here: 653 us
  local copies, waits for them, and re-layouts  313 us (48%)
  waiting for transfers between devices  143 us (22%)
  blocking collectives  117 us (18%)
  loops' own time  25.5 us (4%)
  other arithmetic  20.8 us (3%)
  between operations  14.9 us (2%)
  matrix products  11.7 us (2%)
  starting transfers between devices  7.16 us (1%)
    slice x328, local copies, waits for them, and re-layouts, forward(): lax.associative_scan(combine, (factor_real, factor_imag, push_real, push_...  106 us
    slice x327, local copies, waits for them, and re-layouts, backward(): lax.associative_scan(combine, (factor_real, -factor_imag, pulled_real_par...  106 us
    reduce_scatter x1, waiting for transfers between devices, on_device(): lax.psum_scatter(jnp.einsum('ct,td->cd', picked, tokens, preferred_elemen...  77.7 us
    reduce_scatter x1, waiting for transfers between devices, on_device(): lax.psum_scatter(jnp.einsum('ct,td->cd', picked, cotangent, preferred_ele...  60.7 us
    all_gather x1, blocking collectives, on_device(): lax.all_gather(in_weight, 'sp', axis=0, tiled=True)  45.7 us
    pad x128, local copies, waits for them, and re-layouts, backward(): lax.associative_scan(combine, (factor_real, -factor_imag, pulled_real_par...  41.8 us
    pad x128, local copies, waits for them, and re-layouts, forward(): lax.associative_scan(combine, (factor_real, factor_imag, push_real, push_...  41.8 us
    all_gather x1, blocking collectives, on_device(): lax.all_gather(out_weight, 'sp', axis=0, tiled=True)  38.5 us
  transfers between devices with their start and end apart: 6, of which 3 were waited for; matrix products, arithmetic and copies ran while one was open for 26% of the time, Pallas kernels for 0%

commit v1 on v0

v1 whole, which is shorter than its diff:
```python
import functools

import jax
import jax.numpy as jnp
from jax import lax
from jax.experimental import pallas as pl
from jax.experimental.pallas import tpu as pltpu
from jax.sharding import PartitionSpec as P

MESH = pl.DeviceIdType.MESH
f32 = jnp.float32
bf16 = jnp.bfloat16
LANES = 128


def exact_dot(a, b):
    return jnp.dot(a, b, precision=lax.Precision.HIGHEST, preferred_element_type=f32)


def fast_dot(a, b):
    return jnp.dot(a, b, preferred_element_type=f32)


def dot_nt(a, b):
    return lax.dot_general(a, b, (((1,), (1,)), ((), ())), preferred_element_type=f32)


def dot_tn(a, b):
    return lax.dot_general(a, b, (((0,), (0,)), ((), ())), preferred_element_type=f32)


def kernel(
    sizes,
    tok_ref,
    cot_ref,
    inw_ref,
    outw_ref,
    pack_ref,
    gt_ref,
    giw_ref,
    gow_ref,
    win,
    wout,
    packs,
    btab,
    ctab,
    steps,
    pows,
    skips,
    dps,
    dpr,
    ends_out,
    ends,
    rsb,
    rsr,
    zs,
    zr,
    sz,
    rz,
    sq,
    rq,
    spk,
    rpk,
    sdp,
    rdp,
    sen,
    ren,
    srs,
    rrs,
    szs,
    rzs,
):
    n, nd, n_out, n_in, states, chans, n_groups = sizes
    length = tok_ref.shape[0]
    rows, width = inw_ref.shape
    n_packs = packs.shape[0]
    total_states = n_groups * states
    own_chans = n_groups * chans
    halves = total_states // LANES
    s = lax.axis_index("sp")
    d = lax.axis_index("dp")
    a = s // n_in
    q = lax.rem(s, n_in)

    def remote(src, dst, ssem, rsem, sp, dp):
        return pltpu.make_async_remote_copy(
            src_ref=src,
            dst_ref=dst,
            send_sem=ssem,
            recv_sem=rsem,
            device_id=(sp, dp),
            device_id_type=MESH,
        )

    def outer_at(k):
        return lax.rem(a + k + n_out, n_out)

    def inner_at(j):
        return lax.rem(q + j + n_in, n_in)

    barrier = pltpu.get_barrier_semaphore()
    for k in range(1, n):
        pl.semaphore_signal(barrier, inc=1, device_id=(lax.rem(s + k, n), d), device_id_type=MESH)
    for k in range(1, nd):
        pl.semaphore_signal(barrier, inc=1, device_id=(s, lax.rem(d + k, nd)), device_id_type=MESH)
    pl.semaphore_wait(barrier, n - 1 + nd - 1)

    sent = []

    pack_slot = lax.rem(s, n_packs)
    pack_owner = (s // n_packs) == d

    def pack_copy(k):
        return remote(
            pack_ref, packs.at[pack_slot], spk.at[k], rpk.at[pack_slot], lax.rem(s + k, n), d
        )

    @pl.when(pack_owner)
    def _():
        for k in range(1, n):
            pack_copy(k).start()
        packs[pack_slot] = pack_ref[...]

    owns = (inw_ref, outw_ref)
    bufs = (win, wout)

    def start_gather(w):
        for k in range(1, n_out):
            c = remote(owns[w], bufs[w].at[s], sz.at[w, k], rz.at[w, k], outer_at(k) * n_in + q, d)
            c.start()
            sent.append(c)
        for j in range(1, n_in):
            c = remote(
                owns[w], bufs[w].at[s], sq.at[w, j, 0], rq.at[w, j, 0], a * n_in + inner_at(j), d
            )
            c.start()
            sent.append(c)
        bufs[w][s] = owns[w][...]

    def forward_gather(w):
        for k in range(1, n_out):
            src = outer_at(-k) * n_in + q
            block = bufs[w].at[src]
            remote(block, block, sz.at[w, k], rz.at[w, k], s, d).wait_recv()
            for j in range(1, n_in):
                c = remote(
                    block, block, sq.at[w, j, k], rq.at[w, j, k], a * n_in + inner_at(j), d
                )
                c.start()
                sent.append(c)

    def finish_gather(w):
        for k in range(n_out):
            for j in range(1, n_in):
                block = bufs[w].at[outer_at(-k) * n_in + inner_at(-j)]
                remote(block, block, sq.at[w, j, k], rq.at[w, j, k], s, d).wait_recv()

    start_gather(0)
    start_gather(1)
    forward_gather(0)

    for k in range(n_packs):
        source = d * n_packs + k

        @pl.when(source != s)
        def _():
            remote(packs.at[k], packs.at[k], spk.at[0], rpk.at[k], s, d).wait_recv()

    params = packs[...].reshape(total_states, LANES)

    def spread(column, lanes):
        lane = lax.broadcasted_iota(jnp.int32, (LANES, lanes), 0)
        return exact_dot(params, jnp.where(lane == column, 1.0, 0.0).astype(f32))

    def tiled(first):
        lane = lax.broadcasted_iota(jnp.int32, (LANES, own_chans), 0)
        chan = lax.broadcasted_iota(jnp.int32, (LANES, own_chans), 1)
        return exact_dot(
            params, jnp.where(lane == first + lax.rem(chan, chans), 1.0, 0.0).astype(f32)
        )

    rate, freq = spread(4 * chans, length), spread(4 * chans + 1, length)
    step = jnp.exp(spread(4 * chans + 2, length))
    gains = spread(4 * chans + 3, length)
    skips[...] = gains.reshape(n_groups, states, length)[:, :chans, :].reshape(own_chans, length)
    magnitude = jnp.exp(-rate * step)
    angle = freq * step
    ar = magnitude * jnp.cos(angle)
    ai = magnitude * jnp.sin(angle)
    modulus = rate * rate + freq * freq
    hr = ((-rate * (ar - 1.0) + freq * ai) / modulus)[:, :own_chans]
    hi = ((-freq * (ar - 1.0) - rate * ai) / modulus)[:, :own_chans]
    dr, di = tiled(0), tiled(chans)
    mine = (
        lax.broadcasted_iota(jnp.int32, (total_states, own_chans), 0) // states
        == lax.broadcasted_iota(jnp.int32, (total_states, own_chans), 1) // chans
    )
    top, bottom = pl.ds(0, total_states), pl.ds(total_states, total_states)
    btab[top] = jnp.where(mine, hr * dr - hi * di, 0.0).astype(bf16)
    btab[bottom] = jnp.where(mine, hr * di + hi * dr, 0.0).astype(bf16)
    ctab[top] = jnp.where(mine, tiled(2 * chans), 0.0).astype(bf16)
    ctab[bottom] = jnp.where(mine, -tiled(3 * chans), 0.0).astype(bf16)

    lane = lax.broadcasted_iota(jnp.int32, (total_states, length), 1)
    log_steps = max(1, (length - 1).bit_length())
    fr = br = jnp.ones((total_states, length), f32)
    fi = bi = jnp.zeros((total_states, length), f32)
    up, down = lane + 1, length - lane
    for b in range(length.bit_length()):
        if b < log_steps:
            steps[b, 0] = ar
            steps[b, 1] = ai
        hit = ((up >> b) & 1) == 1
        fr, fi = jnp.where(hit, fr * ar - fi * ai, fr), jnp.where(hit, fr * ai + fi * ar, fi)
        hit = ((down >> b) & 1) == 1
        br, bi = jnp.where(hit, br * ar - bi * ai, br), jnp.where(hit, br * ai + bi * ar, bi)
        ar, ai = ar * ar - ai * ai, 2.0 * ar * ai
    pows[0], pows[1], pows[2], pows[3] = fr, fi, br, bi

    def to_rows(column_of):
        turned = column_of.T
        return turned

    def row_blocks(matrix, at):
        turned = matrix.T[at : at + 1, :]
        return jnp.concatenate([turned[:, h * LANES : (h + 1) * LANES] for h in range(halves)], axis=0)

    jump_r, jump_i = row_blocks(fr, length - 1), row_blocks(fi, length - 1)

    def to_columns(blocks):
        parts = [
            jnp.broadcast_to(blocks[h : h + 1, :], (LANES, LANES)).T for h in range(halves)
        ]
        full = jnp.concatenate(parts, axis=0)
        return jnp.concatenate([full] * (length // LANES), axis=1) if length > LANES else full

    def scan(xr, xi, reverse):
        for b in range(log_steps):
            gap = 1 << b
            mr, mi = steps[b, 0], steps[b, 1]
            if reverse:
                mi = -mi
                keep = lane < length - gap
                shift = length - gap
            else:
                keep = lane >= gap
                shift = gap
            pr = jnp.where(keep, pltpu.roll(xr, shift, 1), 0.0)
            pi = jnp.where(keep, pltpu.roll(xi, shift, 1), 0.0)
            xr, xi = xr + mr * pr - mi * pi, xi + mr * pi + mi * pr
        return xr, xi

    def send_ends(e, xr, xi, at):
        ends_out[e, :halves] = row_blocks(xr, at)
        ends_out[e, halves:] = row_blocks(xi, at)
        for k in range(1, n):
            c = remote(
                ends_out.at[e], ends.at[e, s], sen.at[e, k], ren.at[e, k], lax.rem(s + k, n), d
            )
            c.start()
            sent.append(c)
        ends[e, s] = ends_out[e]

    def carried(e, reverse):
        for k in range(1, n):
            block = ends.at[e, lax.rem(s - k + n, n)]
            remote(block, block, sen.at[e, k], ren.at[e, k], s, d).wait_recv()
        mr = jump_r
        mi = -jump_i if reverse else jump_i
        cr = jnp.zeros((halves, LANES), f32)
        ci = jnp.zeros((halves, LANES), f32)
        for j in range(n - 1, -1, -1) if reverse else range(n):
            use = (s < j) if reverse else (s > j)
            nr = mr * cr - mi * ci + ends[e, j, :halves]
            ni = mr * ci + mi * cr + ends[e, j, halves:]
            cr, ci = jnp.where(use, nr, cr), jnp.where(use, ni, ci)
        return to_columns(cr), to_columns(ci)

    def send_partials(e, part):
        dps[e] = part.astype(bf16).reshape(nd, own_chans, length)
        for k in range(1, nd):
            other = lax.rem(d + k, nd)
            c = remote(dps.at[e, other], dpr.at[e, d], sdp.at[e, k], rdp.at[e, k], s, other)
            c.start()
            sent.append(c)
        dpr[e, d] = dps[e, d]

    def send_share(e, share):
        dpr[e, d] = share
        for k in range(1, nd):
            block = dpr.at[e, d]
            c = remote(block, block, sdp.at[e, k], rdp.at[e, k], s, lax.rem(d + k, nd))
            c.start()
            sent.append(c)

    def wait_shares(e):
        for k in range(1, nd):
            block = dpr.at[e, lax.rem(d - k + nd, nd)]
            remote(block, block, sdp.at[e, k], rdp.at[e, k], s, d).wait_recv()

    def summed(e):
        wait_shares(e)
        total = dpr[e, 0].astype(f32)
        for k in range(1, nd):
            total = total + dpr[e, k].astype(f32)
        return total.astype(bf16)

    def start_reduce(r, part):
        for block in range(n):
            rsb[r, block % n_in, block // n_in] = part[block * rows : (block + 1) * rows].astype(bf16)
        for k in list(range(1, n_out)) + [0]:
            for j in range(1, n_in):
                c = remote(
                    rsb.at[r, inner_at(j), outer_at(k)],
                    rsr.at[r, j, k],
                    srs.at[r, j, k],
                    rrs.at[r, j, k],
                    a * n_in + inner_at(j),
                    d,
                )
                c.start()
                sent.append(c)

    def inner_sum(r, k):
        total = rsb[r, q, outer_at(k)].astype(f32)
        for j in range(1, n_in):
            block = rsr.at[r, j, k]
            remote(block, block, srs.at[r, j, k], rrs.at[r, j, k], s, d).wait_recv()
            total = total + rsr[r, j, k].astype(f32)
        return total

    def forward_reduce(r):
        for k in range(1, n_out):
            zs[r, k] = inner_sum(r, k).astype(bf16)
            c = remote(
                zs.at[r, k], zr.at[r, k], szs.at[r, k], rzs.at[r, k], outer_at(k) * n_in + q, d
            )
            c.start()
            sent.append(c)

    def finish_reduce(r):
        total = inner_sum(r, 0)
        for k in range(1, n_out):
            block = zr.at[r, k]
            remote(block, block, szs.at[r, k], rzs.at[r, k], s, d).wait_recv()
            total = total + zr[r, k].astype(f32)
        return total * (n * length) ** (-0.5)

    forward_gather(1)
    finish_gather(0)
    full_in = win[...].reshape(n * rows, width)
    send_partials(0, dot_nt(full_in, tok_ref[...]))
    drive = summed(0)
    push = fast_dot(btab[...], drive)
    xr, xi = scan(push[:total_states], push[total_states:], False)
    send_ends(0, xr, xi, length - 1)

    finish_gather(1)
    send_partials(1, dot_nt(wout[...].reshape(n * rows, width), cot_ref[...]))
    back = summed(1).astype(f32)

    cr, ci = carried(0, False)
    fr, fi = pows[0], pows[1]
    xr, xi = xr + fr * cr - fi * ci, xi + fr * ci + fi * cr
    mixed = dot_tn(ctab[...], jnp.concatenate([xr, xi], axis=0).astype(bf16))
    mixed = mixed + skips[...] * drive.astype(f32)
    root = 0.7978845608028654
    squared = mixed * mixed
    bent = jnp.tanh(root * mixed * (1.0 + 0.044715 * squared))
    send_share(2, (0.5 * mixed * (1.0 + bent)).astype(bf16))
    slope = 0.5 * (1.0 + bent) + 0.5 * mixed * (1.0 - bent * bent) * root * (
        1.0 + 3.0 * 0.044715 * squared
    )
    inner = slope * back
    pulled = fast_dot(ctab[...], inner.astype(bf16))
    yr, yi = scan(pulled[:total_states], pulled[total_states:], True)
    send_ends(1, yr, yi, 0)

    wait_shares(2)
    start_reduce(0, fast_dot(dpr[2].reshape(n * rows, length), cot_ref[...]))

    cr, ci = carried(1, True)
    br, bi = pows[2], -pows[3]
    yr, yi = yr + br * cr - bi * ci, yi + br * ci + bi * cr
    grad = dot_tn(btab[...], jnp.concatenate([yr, yi], axis=0).astype(bf16))
    send_share(3, (grad + skips[...] * inner).astype(bf16))
    wait_shares(3)
    grad_cols = dpr[3].reshape(n * rows, length)
    start_reduce(1, fast_dot(grad_cols, tok_ref[...]))
    forward_reduce(0)
    gt_ref[...] = dot_tn(grad_cols, win[...].reshape(n * rows, width)).astype(bf16)
    forward_reduce(1)
    gow_ref[...] = finish_reduce(0)
    giw_ref[...] = finish_reduce(1)

    for c in sent:
        c.wait_send()

    @pl.when(pack_owner)
    def _():
        for k in range(1, n):
            pack_copy(k).wait_send()


def solution(mesh):
    n, nd = mesh.shape["sp"], mesh.shape["dp"]
    n_in = 4 if n % 4 == 0 else 1
    n_out = n // n_in

    def on_device(
        tokens,
        cotangent,
        in_weight,
        out_weight,
        decay_rate,
        frequency,
        step_log,
        drive_real,
        drive_imag,
        readout_real_part,
        readout_imaginary,
        skip_gain,
    ):
        length, width = tokens.shape
        rows = in_weight.shape[0]
        groups_here, states, chans = drive_real.shape
        n_groups = groups_here * n // nd
        n_packs = n // nd
        pack = jnp.concatenate(
            [
                drive_real,
                drive_imag,
                jnp.swapaxes(readout_real_part, 1, 2),
                jnp.swapaxes(readout_imaginary, 1, 2),
                decay_rate[..., None],
                frequency[..., None],
                jnp.broadcast_to(step_log[:, None, None], (groups_here, states, 1)),
                jnp.pad(skip_gain, ((0, 0), (0, states - chans)))[..., None],
                jnp.zeros((groups_here, states, LANES - 4 * chans - 4), f32),
            ],
            axis=2,
        ).reshape(groups_here * states, LANES)
        total_states = n_groups * states
        own_chans = n_groups * chans
        end_rows = 2 * total_states // LANES
        log_steps = max(1, (length - 1).bit_length())
        dma = pltpu.SemaphoreType.DMA
        vmem = pl.BlockSpec(memory_space=pltpu.VMEM)
        return pl.pallas_call(
            functools.partial(kernel, (n, nd, n_out, n_in, states, chans, n_groups)),
            out_shape=(
                jax.ShapeDtypeStruct((length, width), bf16),
                jax.ShapeDtypeStruct((rows, width), f32),
                jax.ShapeDtypeStruct((rows, width), f32),
            ),
            in_specs=[vmem] * 5,
            out_specs=(vmem,) * 3,
            scratch_shapes=[
                pltpu.VMEM((n, rows, width), bf16),
                pltpu.VMEM((n, rows, width), bf16),
                pltpu.VMEM((n_packs, groups_here * states, LANES), f32),
                pltpu.VMEM((2 * total_states, own_chans), bf16),
                pltpu.VMEM((2 * total_states, own_chans), bf16),
                pltpu.VMEM((log_steps, 2, total_states, length), f32),
                pltpu.VMEM((4, total_states, length), f32),
                pltpu.VMEM((own_chans, length), f32),
                pltpu.VMEM((2, nd, own_chans, length), bf16),
                pltpu.VMEM((4, nd, own_chans, length), bf16),
                pltpu.VMEM((2, end_rows, LANES), f32),
                pltpu.VMEM((2, n, end_rows, LANES), f32),
                pltpu.VMEM((2, n_in, n_out, rows, width), bf16),
                pltpu.VMEM((2, n_in, n_out, rows, width), bf16),
                pltpu.VMEM((2, n_out, rows, width), bf16),
                pltpu.VMEM((2, n_out, rows, width), bf16),
                dma((2, n_out)),
                dma((2, n_out)),
                dma((2, n_in, n_out)),
                dma((2, n_in, n_out)),
                dma((n,)),
                dma((n_packs,)),
                dma((4, nd)),
                dma((4, nd)),
                dma((2, n)),
                dma((2, n)),
                dma((2, n_in, n_out)),
                dma((2, n_in, n_out)),
                dma((2, n_out)),
                dma((2, n_out)),
            ],
            compiler_params=pltpu.CompilerParams(
                collective_id=0, has_side_effects=True, vmem_limit_bytes=48 * 1024 * 1024
            ),
        )(tokens, cotangent, in_weight, out_weight, pack)

    return jax.shard_map(
        on_device,
        mesh=mesh,
        in_specs=(
            P("sp", "dp"),
            P("sp", "dp"),
            P("sp", "dp"),
            P("sp", "dp"),
            P("sp", None),
            P("sp", None),
            P("sp"),
            P("sp", None, None),
            P("sp", None, None),
            P("sp", None, None),
            P("sp", None, None),
            P("sp", None),
        ),
        out_specs=(P("sp", "dp"), P("sp", "dp"), P("sp", "dp")),
        check_vma=False,
    )
```

time: 657 us -> 55.8 us (0.08)
  local copies, waits for them, and re-layouts: 313 us -> 8.98 us
  waiting for transfers between devices: 143 us -> 0 us
  blocking collectives: 117 us -> 0 us
  Pallas kernels: 0 us -> 45 us
  loops' own time: 25.5 us -> 0 us
  other arithmetic: 20.8 us -> 0 us
  between operations: 14.9 us -> 1.36 us
  matrix products: 11.7 us -> 0 us
  starting transfers between devices: 7.16 us -> 0 us
    slice x655 -> x0, local copies, waits for them, and re-layouts: 213 us -> none  [the longest x328 106 us: forward(): lax.associative_scan(combine, (factor_real, factor_imag, push_real, push_...]
    reduce_scatter x4 -> x0, waiting for transfers between devices: 138 us -> none  [the longest x1 77.7 us: on_device(): lax.psum_scatter(jnp.einsum('ct,td->cd', picked, tokens, preferred_elemen...]
    all_gather x6 -> x0, blocking collectives: 92.3 us -> none  [the longest x1 45.7 us: on_device(): lax.all_gather(in_weight, 'sp', axis=0, tiled=True)]
    pad x256 -> x0, local copies, waits for them, and re-layouts: 83.6 us -> none  [the longest x128 41.8 us: backward(): lax.associative_scan(combine, (factor_real, -factor_imag, pulled_real_par...]
    pallas_call x0 -> x1, Pallas kernels: none -> 45 us  [on_device(): pl.pallas_call(functools.partial(kernel, (n, nd, n_out, n_in, states, cha...]
    another operation x2 -> x0, loops' own time: 25.5 us -> none  [the longest x1 21.6 us: mechanism(): lax.scan(backward, (empty_state, empty_state), (mixed_blocks, to_blocks(h...]
    all_to_all x2 -> x0, blocking collectives: 24.2 us -> none  [the longest x1 14.1 us: on_device(): lax.all_to_all(gated_slice, 'sp', split_axis=1, concat_axis=0, tiled=True)]
    dot_general x37 -> x0, matrix products: 11.7 us -> none  [the longest x1 1.29 us: on_device(): jnp.einsum('ct,td->cd', picked, tokens, preferred_element_type=jnp.float32)]
  transfers between devices with their start and end apart: 6 -> 0, of which waited for: 3 -> 0; matrix products, arithmetic and copies ran while one was open for 26% -> 0% of each run, Pallas kernels for 0% -> 0%
where the time goes in v1:
time: 55.8 us; the launch traced here: 55.4 us
  Pallas kernels  45 us (81%)
  local copies, waits for them, and re-layouts  8.98 us (16%)
  between operations  1.36 us (2%)
    pallas_call x1, Pallas kernels, on_device(): pl.pallas_call(functools.partial(kernel, (n, nd, n_out, n_in, states, cha...  45 us
    unnamed x15, local copies, waits for them, and re-layouts  6.66 us

profile of v1, /device:TPU:0, one launch (start us, length us, event | category | flops | bytes accessed | tf_op | source)
XLA Modules:
  0.0 55.4 jit_solution(11430959527047080998)
XLA Ops:
  0.6 0.0 copy-start
  1.3 0.7 %pad_bitcast_fusion = f32[1,32,1]{1,2,0:T(1,128)S(1)} fusion(f32[1,16]{1,0:T(1,128)} %param.23), kind=kLoop, calls=%fused_computation | loop fusion | bytes 192 | tf_op jit(solution)/shard_map/broadcast_in_dim | solution.py:438
  2.0 0.1 copy.21
  2.1 0.7 %copy.19 = f32[1,32,1]{2,1,0:T(8,128)S(1)} copy(f32[1,32,1]{1,2,0:T(1,128)} %bitcast.12) | data formatting | bytes 256 | tf_op jit(solution)/shard_map/broadcast_in_dim | solution.py:435
  2.8 0.7 %copy.20 = f32[1,32,1]{2,1,0:T(8,128)S(1)} copy(f32[1,32,1]{1,2,0:T(1,128)} %bitcast.13) | data formatting | bytes 256 | tf_op jit(solution)/shard_map/broadcast_in_dim | solution.py:436
  3.6 0.8 %copy.17 = f32[1,32,16]{2,1,0:T(8,128)S(1)} copy(f32[1,32,16]{1,2,0:T(8,128)} %param.19) | data formatting | bytes 4096 | tf_op args[7]
  4.3 0.8 %copy.18 = f32[1,32,16]{2,1,0:T(8,128)S(1)} copy(f32[1,32,16]{1,2,0:T(8,128)} %param.20) | data formatting | bytes 4096 | tf_op args[8]
  5.1 0.8 %copy.15 = f32[1,16,32]{1,2,0:T(8,128)S(1)} copy(f32[1,16,32]{2,1,0:T(8,128)} %param.21) | data formatting | bytes 4096 | tf_op args[9]
  5.9 0.8 %copy.16 = f32[1,16,32]{1,2,0:T(8,128)S(1)} copy(f32[1,16,32]{2,1,0:T(8,128)} %param.22) | data formatting | bytes 4096 | tf_op args[10]
  6.6 0.0 copy-start.2
  6.6 0.0 copy-start.3
  6.6 0.1 concatenate.3
  6.8 0.0 copy-done
  6.8 0.6 %copy-done.2 = bf16[16,1024]{1,0:T(8,128)(2,1)S(1)} copy-done((bf16[16,1024]{1,0:T(8,128)(2,1)S(1)}, bf16[16,1024]{1,0:T(8,128)(2,1)}, u32[]{:S(2)}) %copy-start.2) | copy-done | bytes 32792
  7.4 0.0 copy-done.3
  7.4 0.0 copy-start.1
  7.4 0.9 %copy-done.1 = bf16[128,1024]{1,0:T(8,128)(2,1)S(1)} copy-done((bf16[128,1024]{1,0:T(8,128)(2,1)S(1)}, bf16[128,1024]{1,0:T(8,128)(2,1)}, u32[]{:S(2)}) %copy-start.1) | copy-done | bytes 262168
  8.4 45.0 %shard_map.139 = (bf16[128,1024]{1,0:T(8,128)(2,1)S(1)}, f32[16,1024]{1,0:T(8,128)S(1)}, f32[16,1024]{1,0:T(8,128)S(1)}) custom-call(bf16[128,1024]{1,0:T(8,128)(2,1)S(1)} %copy-done, bf16[128,1024]{1,0:T(8,128)(2,1)S(1)} %copy-done.1, bf16[16,1024]{1,0:T(8,128)(2,1)S(1)} %copy-done.2, bf16[16,1024]{1,0:T(8,128)(2,1)S(1)} %copy-done.3, f32[32,128]{1,0:T(8,128)S(1)} %bitcast.9), custom_call_target="tpu_custom_call" | custom-call | tf_op jit(solution)/shard_map/pallas_call | solution.py:449
  53.4 0.7 %copy.26 = bf16[128,1024]{1,0:T(8,128)(2,1)} copy(bf16[128,1024]{1,0:T(8,128)(2,1)S(1)} %get-tuple-element.6) | data formatting | bytes 524288
  54.1 0.6 %copy.27 = f32[16,1024]{1,0:T(8,128)} copy(f32[16,1024]{1,0:T(8,128)S(1)} %get-tuple-element.7) | data formatting | bytes 131072
  54.7 0.6 %copy.28 = f32[16,1024]{1,0:T(8,128)} copy(f32[16,1024]{1,0:T(8,128)S(1)} %get-tuple-element.8) | data formatting | bytes 131072
  (2 shorter events, 0.0 us)
Async XLA Ops:
  0.6 6.1 %copy-start = (bf16[128,1024]{1,0:T(8,128)(2,1)S(1)}, bf16[128,1024]{1,0:T(8,128)(2,1)}, u32[]{:S(2)}) copy-start(bf16[128,1024]{1,0:T(8,128)(2,1)} %tok_ref.1) | copy-start | bytes 786436
  6.6 0.8 %copy-start.2 = (bf16[16,1024]{1,0:T(8,128)(2,1)S(1)}, bf16[16,1024]{1,0:T(8,128)(2,1)}, u32[]{:S(2)}) copy-start(bf16[16,1024]{1,0:T(8,128)(2,1)} %inw_ref.1) | copy-start | bytes 98308
  6.6 0.8 %copy-start.3 = (bf16[16,1024]{1,0:T(8,128)(2,1)S(1)}, bf16[16,1024]{1,0:T(8,128)(2,1)}, u32[]{:S(2)}) copy-start(bf16[16,1024]{1,0:T(8,128)(2,1)} %outw_ref.1) | copy-start | bytes 98308
  7.4 0.9 %copy-start.1 = (bf16[128,1024]{1,0:T(8,128)(2,1)S(1)}, bf16[128,1024]{1,0:T(8,128)(2,1)}, u32[]{:S(2)}) copy-start(bf16[128,1024]{1,0:T(8,128)(2,1)} %cot_ref.1) | copy-start | bytes 786436

commit v2 on v1

--- a/solution.py
+++ b/solution.py
@@ -21,6 +21,16 @@
     return jnp.dot(a, b, preferred_element_type=f32)
 
 
+def exact_tn(a, b):
+    return lax.dot_general(
+        a,
+        b,
+        (((0,), (0,)), ((), ())),
+        precision=lax.Precision.HIGHEST,
+        preferred_element_type=f32,
+    )
+
+
 def dot_nt(a, b):
     return lax.dot_general(a, b, (((1,), (1,)), ((), ())), preferred_element_type=f32)
 
@@ -31,14 +41,30 @@
 
 def kernel(
     sizes,
+    tok_hbm,
+    cot_hbm,
+    inw_hbm,
+    outw_hbm,
+    rate_hbm,
+    freq_hbm,
+    step_ref,
+    dr_hbm,
+    di_hbm,
+    ror_hbm,
+    roi_hbm,
+    skip_hbm,
+    gt_ref,
+    grads_ref,
     tok_ref,
     cot_ref,
-    inw_ref,
-    outw_ref,
+    rate_ref,
+    freq_ref,
+    dr_ref,
+    di_ref,
+    ror_ref,
+    roi_ref,
+    skip_ref,
     pack_ref,
-    gt_ref,
-    giw_ref,
-    gow_ref,
     win,
     wout,
     packs,
@@ -55,12 +81,11 @@
     rsr,
     zs,
     zr,
+    loads,
     sz,
     rz,
     sq,
     rq,
-    spk,
-    rpk,
     sdp,
     rdp,
     sen,
@@ -72,7 +97,7 @@
 ):
     n, nd, n_out, n_in, states, chans, n_groups = sizes
     length = tok_ref.shape[0]
-    rows, width = inw_ref.shape
+    rows, width = inw_hbm.shape
     n_packs = packs.shape[0]
     total_states = n_groups * states
     own_chans = n_groups * chans
@@ -98,74 +123,154 @@
     def inner_at(j):
         return lax.rem(q + j + n_in, n_in)
 
+    bufs = (win, wout)
+    load_in = pltpu.make_async_copy(inw_hbm, win.at[s], loads.at[0])
+    load_out = pltpu.make_async_copy(outw_hbm, wout.at[s], loads.at[1])
+    load_tok = pltpu.make_async_copy(tok_hbm, tok_ref, loads.at[2])
+    load_cot = pltpu.make_async_copy(cot_hbm, cot_ref, loads.at[3])
+    params_in = (
+        (rate_hbm, rate_ref),
+        (freq_hbm, freq_ref),
+        (dr_hbm, dr_ref),
+        (di_hbm, di_ref),
+        (ror_hbm, ror_ref),
+        (roi_hbm, roi_ref),
+        (skip_hbm, skip_ref),
+    )
+    load_params = [
+        pltpu.make_async_copy(there, here, loads.at[4 + i])
+        for i, (there, here) in enumerate(params_in)
+    ]
+    for load in load_params + [load_in, load_out, load_tok, load_cot]:
+        load.start()
+
     barrier = pltpu.get_barrier_semaphore()
     for k in range(1, n):
         pl.semaphore_signal(barrier, inc=1, device_id=(lax.rem(s + k, n), d), device_id_type=MESH)
     for k in range(1, nd):
         pl.semaphore_signal(barrier, inc=1, device_id=(s, lax.rem(d + k, nd)), device_id_type=MESH)
-    pl.semaphore_wait(barrier, n - 1 + nd - 1)
+
+    def place(count, first):
+        lane = lax.broadcasted_iota(jnp.int32, (count, LANES), 1)
+        return jnp.where(lane == first + lax.broadcasted_iota(jnp.int32, (count, LANES), 0), 1.0, 0.0)
+
+    def place_row(row, column):
+        spot = lax.broadcasted_iota(jnp.int32, (8, LANES), 0) == 0
+        spot = spot & (lax.broadcasted_iota(jnp.int32, (8, LANES), 1) == column)
+        return exact_tn(jnp.broadcast_to(row, (8, row.shape[1])), jnp.where(spot, 1.0, 0.0))
+
+    for load in load_params:
+        load.wait()
+    for g in range(dr_ref.shape[0]):
+        spots = [place(chans, m * chans) for m in range(4)]
+        block = exact_tn(dr_ref[g], spots[0]) + exact_tn(di_ref[g], spots[1])
+        block = block + exact_tn(ror_ref[g], spots[2]) + exact_tn(roi_ref[g], spots[3])
+        block = block + place_row(rate_ref[g : g + 1, :], 4 * chans)
+        block = block + place_row(freq_ref[g : g + 1, :], 4 * chans + 1)
+        lane = lax.broadcasted_iota(jnp.int32, (states, LANES), 1)
+        block = block + jnp.where(lane == 4 * chans + 2, step_ref[g], 0.0)
+        gain = place_row(skip_ref[g : g + 1, :], 4 * chans + 3)
+        pack_ref[g * states : g * states + chans] = block[:chans] + gain
+        pack_ref[g * states + chans : (g + 1) * states] = block[chans:]
+    with jax.named_scope("barrier"):
+        pl.semaphore_wait(barrier, n - 1 + nd - 1)
 
     sent = []
 
-    pack_slot = lax.rem(s, n_packs)
-    pack_owner = (s // n_packs) == d
-
-    def pack_copy(k):
-        return remote(
-            pack_ref, packs.at[pack_slot], spk.at[k], rpk.at[pack_slot], lax.rem(s + k, n), d
-        )
-
-    @pl.when(pack_owner)
-    def _():
-        for k in range(1, n):
-            pack_copy(k).start()
-        packs[pack_slot] = pack_ref[...]
-
-    owns = (inw_ref, outw_ref)
-    bufs = (win, wout)
-
-    def start_gather(w):
-        for k in range(1, n_out):
-            c = remote(owns[w], bufs[w].at[s], sz.at[w, k], rz.at[w, k], outer_at(k) * n_in + q, d)
-            c.start()
-            sent.append(c)
-        for j in range(1, n_in):
-            c = remote(
-                owns[w], bufs[w].at[s], sq.at[w, j, 0], rq.at[w, j, 0], a * n_in + inner_at(j), d
-            )
-            c.start()
-            sent.append(c)
-        bufs[w][s] = owns[w][...]
+    def when_used(w, src, act):
+        if w == 2:
+            pl.when(src // n_packs == d)(act)
+        else:
+            act()
+
+    def slot(w, src):
+        return packs.at[lax.rem(src, n_packs)] if w == 2 else bufs[w].at[src]
+
+    def own(w):
+        return pack_ref if w == 2 else bufs[w].at[s]
+
+    def outer_copy(w, k):
+        return remote(own(w), slot(w, s), sz.at[w, k], rz.at[w, k], outer_at(k) * n_in + q, d)
+
+    def inner_copy(w, j, k):
+        src = outer_at(-k) * n_in + q
+        block = own(w) if k == 0 else slot(w, src)
+        peer = a * n_in + inner_at(j)
+        return remote(block, slot(w, src), sq.at[w, j, k], rq.at[w, j, k], peer, d)
+
+    def send_outer(w):
+        def act():
+            for k in range(1, n_out):
+                outer_copy(w, k).start()
+
+        when_used(w, s, act)
+
+    def send_inner(w):
+        def act():
+            for j in range(1, n_in):
+                inner_copy(w, j, 0).start()
+
+        when_used(w, s, act)
 
     def forward_gather(w):
         for k in range(1, n_out):
             src = outer_at(-k) * n_in + q
-            block = bufs[w].at[src]
-            remote(block, block, sz.at[w, k], rz.at[w, k], s, d).wait_recv()
-            for j in range(1, n_in):
-                c = remote(
-                    block, block, sq.at[w, j, k], rq.at[w, j, k], a * n_in + inner_at(j), d
-                )
-                c.start()
-                sent.append(c)
+
+            def act():
+                block = slot(w, src)
+                remote(block, block, sz.at[w, k], rz.at[w, k], s, d).wait_recv()
+                for j in range(1, n_in):
+                    inner_copy(w, j, k).start()
+
+            when_used(w, src, act)
 
     def finish_gather(w):
         for k in range(n_out):
             for j in range(1, n_in):
-                block = bufs[w].at[outer_at(-k) * n_in + inner_at(-j)]
-                remote(block, block, sq.at[w, j, k], rq.at[w, j, k], s, d).wait_recv()
-
-    start_gather(0)
-    start_gather(1)
-    forward_gather(0)
-
-    for k in range(n_packs):
-        source = d * n_packs + k
-
-        @pl.when(source != s)
+                src = outer_at(-k) * n_in + inner_at(-j)
+
+                def act():
+                    block = slot(w, src)
+                    remote(block, block, sq.at[w, j, k], rq.at[w, j, k], s, d).wait_recv()
+
+                when_used(w, src, act)
+
+    def drain_gather(w):
+        for k in range(n_out):
+
+            def act():
+                if k:
+                    outer_copy(w, k).wait_send()
+
+            when_used(w, s, act)
+
+            def act():
+                for j in range(1, n_in):
+                    inner_copy(w, j, k).wait_send()
+
+            when_used(w, outer_at(-k) * n_in + q, act)
+
+    with jax.named_scope("starts"):
+        send_outer(2)
+        send_inner(2)
+        load_in.wait()
+        send_outer(0)
+        send_inner(0)
+        load_out.wait()
+        send_outer(1)
+
+        @pl.when(s // n_packs == d)
         def _():
-            remote(packs.at[k], packs.at[k], spk.at[0], rpk.at[k], s, d).wait_recv()
-
+            packs[lax.rem(s, n_packs)] = pack_ref[...]
+
+    with jax.named_scope("fwd2"):
+        forward_gather(2)
+    with jax.named_scope("fwd0"):
+        forward_gather(0)
+    send_inner(1)
+
+    with jax.named_scope("fin2"):
+        finish_gather(2)
     params = packs[...].reshape(total_states, LANES)
 
     def spread(column, lanes):
@@ -217,10 +322,6 @@
         ar, ai = ar * ar - ai * ai, 2.0 * ar * ai
     pows[0], pows[1], pows[2], pows[3] = fr, fi, br, bi
 
-    def to_rows(column_of):
-        turned = column_of.T
-        return turned
-
     def row_blocks(matrix, at):
         turned = matrix.T[at : at + 1, :]
         return jnp.concatenate([turned[:, h * LANES : (h + 1) * LANES] for h in range(halves)], axis=0)
@@ -344,22 +445,33 @@
             block = zr.at[r, k]
             remote(block, block, szs.at[r, k], rzs.at[r, k], s, d).wait_recv()
             total = total + zr[r, k].astype(f32)
-        return total * (n * length) ** (-0.5)
-
-    forward_gather(1)
-    finish_gather(0)
+        return total
+
+    with jax.named_scope("fwd1"):
+        forward_gather(1)
+    with jax.named_scope("fin0"):
+        finish_gather(0)
+    load_tok.wait()
+    load_cot.wait()
     full_in = win[...].reshape(n * rows, width)
-    send_partials(0, dot_nt(full_in, tok_ref[...]))
-    drive = summed(0)
-    push = fast_dot(btab[...], drive)
-    xr, xi = scan(push[:total_states], push[total_states:], False)
-    send_ends(0, xr, xi, length - 1)
-
-    finish_gather(1)
-    send_partials(1, dot_nt(wout[...].reshape(n * rows, width), cot_ref[...]))
-    back = summed(1).astype(f32)
-
-    cr, ci = carried(0, False)
+    with jax.named_scope("proj0"):
+        send_partials(0, dot_nt(full_in, tok_ref[...]))
+    with jax.named_scope("dp0"):
+        drive = summed(0)
+    with jax.named_scope("scan0"):
+        push = fast_dot(btab[...], drive)
+        xr, xi = scan(push[:total_states], push[total_states:], False)
+        send_ends(0, xr, xi, length - 1)
+
+    with jax.named_scope("fin1"):
+        finish_gather(1)
+    with jax.named_scope("proj1"):
+        send_partials(1, dot_nt(wout[...].reshape(n * rows, width), cot_ref[...]))
+    with jax.named_scope("dp1"):
+        back = summed(1).astype(f32)
+
+    with jax.named_scope("carry0"):
+        cr, ci = carried(0, False)
     fr, fi = pows[0], pows[1]
     xr, xi = xr + fr * cr - fi * ci, xi + fr * ci + fi * cr
     mixed = dot_tn(ctab[...], jnp.concatenate([xr, xi], axis=0).astype(bf16))
@@ -376,30 +488,38 @@
     yr, yi = scan(pulled[:total_states], pulled[total_states:], True)
     send_ends(1, yr, yi, 0)
 
-    wait_shares(2)
-    start_reduce(0, fast_dot(dpr[2].reshape(n * rows, length), cot_ref[...]))
-
-    cr, ci = carried(1, True)
+    with jax.named_scope("dp2"):
+        wait_shares(2)
+    with jax.named_scope("rs0"):
+        start_reduce(0, fast_dot(dpr[2].reshape(n * rows, length), cot_ref[...]))
+
+    with jax.named_scope("carry1"):
+        cr, ci = carried(1, True)
     br, bi = pows[2], -pows[3]
     yr, yi = yr + br * cr - bi * ci, yi + br * ci + bi * cr
     grad = dot_tn(btab[...], jnp.concatenate([yr, yi], axis=0).astype(bf16))
     send_share(3, (grad + skips[...] * inner).astype(bf16))
-    wait_shares(3)
+    with jax.named_scope("dp3"):
+        wait_shares(3)
     grad_cols = dpr[3].reshape(n * rows, length)
-    start_reduce(1, fast_dot(grad_cols, tok_ref[...]))
-    forward_reduce(0)
-    gt_ref[...] = dot_tn(grad_cols, win[...].reshape(n * rows, width)).astype(bf16)
-    forward_reduce(1)
-    gow_ref[...] = finish_reduce(0)
-    giw_ref[...] = finish_reduce(1)
+    with jax.named_scope("rs1"):
+        start_reduce(1, fast_dot(grad_cols, tok_ref[...]))
+    with jax.named_scope("frs0"):
+        forward_reduce(0)
+    with jax.named_scope("gt"):
+        gt_ref[...] = dot_tn(grad_cols, win[...].reshape(n * rows, width)).astype(bf16)
+    with jax.named_scope("frs1"):
+        forward_reduce(1)
+    with jax.named_scope("fin_rs0"):
+        grads_ref[1] = finish_reduce(0)
+    with jax.named_scope("fin_rs1"):
+        grads_ref[0] = finish_reduce(1)
 
     for c in sent:
         c.wait_send()
 
-    @pl.when(pack_owner)
-    def _():
-        for k in range(1, n):
-            pack_copy(k).wait_send()
+    for w in range(3):
+        drain_gather(w)
 
 
 def solution(mesh):
@@ -426,36 +546,33 @@
         groups_here, states, chans = drive_real.shape
         n_groups = groups_here * n // nd
         n_packs = n // nd
-        pack = jnp.concatenate(
-            [
-                drive_real,
-                drive_imag,
-                jnp.swapaxes(readout_real_part, 1, 2),
-                jnp.swapaxes(readout_imaginary, 1, 2),
-                decay_rate[..., None],
-                frequency[..., None],
-                jnp.broadcast_to(step_log[:, None, None], (groups_here, states, 1)),
-                jnp.pad(skip_gain, ((0, 0), (0, states - chans)))[..., None],
-                jnp.zeros((groups_here, states, LANES - 4 * chans - 4), f32),
-            ],
-            axis=2,
-        ).reshape(groups_here * states, LANES)
         total_states = n_groups * states
         own_chans = n_groups * chans
         end_rows = 2 * total_states // LANES
         log_steps = max(1, (length - 1).bit_length())
         dma = pltpu.SemaphoreType.DMA
         vmem = pl.BlockSpec(memory_space=pltpu.VMEM)
-        return pl.pallas_call(
+        anywhere = pl.BlockSpec(memory_space=pl.ANY)
+        scale = (n * length) ** (-0.5)
+        grad_tokens, grads = pl.pallas_call(
             functools.partial(kernel, (n, nd, n_out, n_in, states, chans, n_groups)),
             out_shape=(
-                jax.ShapeDtypeStruct((length, width), bf16),
-                jax.ShapeDtypeStruct((rows, width), f32),
-                jax.ShapeDtypeStruct((rows, width), f32),
+                pltpu.VMEM((length, width), bf16),
+                pltpu.VMEM((2, rows, width), f32),
             ),
-            in_specs=[vmem] * 5,
-            out_specs=(vmem,) * 3,
+            in_specs=[anywhere] * 6 + [pl.BlockSpec(memory_space=pltpu.SMEM)] + [anywhere] * 5,
+            out_specs=(vmem,) * 2,
             scratch_shapes=[
+                pltpu.VMEM((length, width), bf16),
+                pltpu.VMEM((length, width), bf16),
+                pltpu.VMEM((groups_here, states), f32),
+                pltpu.VMEM((groups_here, states), f32),
+                pltpu.VMEM((groups_here, chans, states), f32),
+                pltpu.VMEM((groups_here, chans, states), f32),
+                pltpu.VMEM((groups_here, chans, states), f32),
+                pltpu.VMEM((groups_here, chans, states), f32),
+                pltpu.VMEM((groups_here, chans), f32),
+                pltpu.VMEM((groups_here * states, LANES), f32),
                 pltpu.VMEM((n, rows, width), bf16),
                 pltpu.VMEM((n, rows, width), bf16),
                 pltpu.VMEM((n_packs, groups_here * states, LANES), f32),
@@ -472,12 +589,11 @@
                 pltpu.VMEM((2, n_in, n_out, rows, width), bf16),
                 pltpu.VMEM((2, n_out, rows, width), bf16),
                 pltpu.VMEM((2, n_out, rows, width), bf16),
-                dma((2, n_out)),
-                dma((2, n_out)),
-                dma((2, n_in, n_out)),
-                dma((2, n_in, n_out)),
-                dma((n,)),
-                dma((n_packs,)),
+                dma((11,)),
+                dma((3, n_out)),
+                dma((3, n_out)),
+                dma((3, n_in, n_out)),
+                dma((3, n_in, n_out)),
                 dma((4, nd)),
                 dma((4, nd)),
                 dma((2, n)),
@@ -488,9 +604,23 @@
                 dma((2, n_out)),
             ],
             compiler_params=pltpu.CompilerParams(
-                collective_id=0, has_side_effects=True, vmem_limit_bytes=48 * 1024 * 1024
+                collective_id=0, has_side_effects=True, vmem_limit_bytes=67043328 - 4 * 1024 * 1024
             ),
-        )(tokens, cotangent, in_weight, out_weight, pack)
+        )(
+            tokens,
+            cotangent,
+            in_weight,
+            out_weight,
+            decay_rate,
+            frequency,
+            step_log,
+            jnp.swapaxes(drive_real, 1, 2),
+            jnp.swapaxes(drive_imag, 1, 2),
+            readout_real_part,
+            readout_imaginary,
+            skip_gain,
+        )
+        return grad_tokens, grads[0] * scale, grads[1] * scale
 
     return jax.shard_map(
         on_device,

time: 55.8 us -> 47.1 us (0.84)
  local copies, waits for them, and re-layouts: 8.98 us -> 0.71 us
  Pallas kernels: 45 us -> 44.3 us
  other arithmetic: 0 us -> 0.66 us
    unnamed x15 -> x1, local copies, waits for them, and re-layouts: 6.66 us -> 0.71 us
    broadcast_in_dim x6 -> x0, local copies, waits for them, and re-layouts: 2.22 us -> none  [the longest x2 0.75 us: on_device(): jnp.pad(skip_gain, ((0, 0), (0, states - chans)))[..., None]]
    pallas_call x1, Pallas kernels: 45 us -> 44.3 us  [on_device(): pl.pallas_call(functools.partial(kernel, (n, nd, n_out, n_in, states, cha...]
    mul x0 -> x1, other arithmetic: none -> 0.66 us  [on_device(): return (grad_tokens, grads[0] * scale, grads[1] * scale)]
where the time goes in v2:
time: 47.1 us; the launch traced here: 46.9 us
  Pallas kernels  44.3 us (94%)
  between operations  1.29 us (3%)
  local copies, waits for them, and re-layouts  0.71 us (2%)
  other arithmetic  0.66 us (1%)
    pallas_call x1, Pallas kernels, on_device(): pl.pallas_call(functools.partial(kernel, (n, nd, n_out, n_in, states, cha...  44.3 us

profile of v2, /device:TPU:0, one launch (start us, length us, event | category | flops | bytes accessed | tf_op | source)
XLA Modules:
  0.0 46.9 jit_solution(1827523767690306277)
XLA Ops:
  1.3 44.3 %shard_map.139 = (bf16[128,1024]{1,0:T(8,128)(2,1)S(1)}, f32[2,16,1024]{2,1,0:T(8,128)S(1)}) custom-call(bf16[128,1024]{1,0:T(8,128)(2,1)} %tok_hbm.1, bf16[128,1024]{1,0:T(8,128)(2,1)} %cot_hbm.1, bf16[16,1024]{1,0:T(8,128)(2,1)} %inw_hbm.1, bf16[16,1024]{1,0:T(8,128)(2,1)} %outw_hbm.1, f32[1,32]{1,0:T(1,128)} %rate_hbm.1, f32[1,32]{1,0:T(1,128)} %freq_hbm.1, ...), custom_call_target="tpu_custom_call" | custom-call | tf_op jit(solution)/shard_map/pallas_call | solution.py:557
  45.5 0.7 %copy.16 = bf16[128,1024]{1,0:T(8,128)(2,1)} copy(bf16[128,1024]{1,0:T(8,128)(2,1)S(1)} %get-tuple-element.9) | data formatting | bytes 524288
  46.3 0.7 %multiply_bitcast_fusion = (f32[16,1024]{1,0:T(8,128)}, f32[16,1024]{1,0:T(8,128)}) fusion(f32[2,16,1024]{2,1,0:T(8,128)S(1)} %get-tuple-element.6), kind=kLoop, calls=%fused_computation | loop fusion | flops 32768 | bytes 262144 | tf_op jit(solution)/shard_map/mul | solution.py:623

commit v3 on v2

--- a/solution.py
+++ b/solution.py
@@ -306,6 +306,8 @@
     ctab[top] = jnp.where(mine, tiled(2 * chans), 0.0).astype(bf16)
     ctab[bottom] = jnp.where(mine, -tiled(3 * chans), 0.0).astype(bf16)
 
+    with jax.named_scope("fwd1"):
+        forward_gather(1)
     lane = lax.broadcasted_iota(jnp.int32, (total_states, length), 1)
     log_steps = max(1, (length - 1).bit_length())
     fr = br = jnp.ones((total_states, length), f32)
@@ -447,8 +449,6 @@
             total = total + zr[r, k].astype(f32)
         return total
 
-    with jax.named_scope("fwd1"):
-        forward_gather(1)
     with jax.named_scope("fin0"):
         finish_gather(0)
     load_tok.wait()

time: 47.1 us -> 46.6 us (0.989)
  Pallas kernels: 44.3 us -> 43.8 us
    pallas_call x1, Pallas kernels: 44.3 us -> 43.8 us  [on_device(): pl.pallas_call(functools.partial(kernel, (n, nd, n_out, n_in, states, cha...]
where the time goes in v3:
time: 46.6 us; the launch traced here: 46.4 us
  Pallas kernels  43.8 us (94%)
  between operations  1.29 us (3%)
  local copies, waits for them, and re-layouts  0.71 us (2%)
  other arithmetic  0.66 us (1%)
    pallas_call x1, Pallas kernels, on_device(): pl.pallas_call(functools.partial(kernel, (n, nd, n_out, n_in, states, cha...  43.8 us

profile of v3, /device:TPU:0, one launch (start us, length us, event | category | flops | bytes accessed | tf_op | source)
XLA Modules:
  0.0 46.4 jit_solution(14836029390312325696)
XLA Ops:
  1.3 43.8 %shard_map.139 = (bf16[128,1024]{1,0:T(8,128)(2,1)S(1)}, f32[2,16,1024]{2,1,0:T(8,128)S(1)}) custom-call(bf16[128,1024]{1,0:T(8,128)(2,1)} %tok_hbm.1, bf16[128,1024]{1,0:T(8,128)(2,1)} %cot_hbm.1, bf16[16,1024]{1,0:T(8,128)(2,1)} %inw_hbm.1, bf16[16,1024]{1,0:T(8,128)(2,1)} %outw_hbm.1, f32[1,32]{1,0:T(1,128)} %rate_hbm.1, f32[1,32]{1,0:T(1,128)} %freq_hbm.1, ...), custom_call_target="tpu_custom_call" | custom-call | tf_op jit(solution)/shard_map/pallas_call | solution.py:557
  45.1 0.7 %copy.16 = bf16[128,1024]{1,0:T(8,128)(2,1)} copy(bf16[128,1024]{1,0:T(8,128)(2,1)S(1)} %get-tuple-element.9) | data formatting | bytes 524288
  45.8 0.7 %multiply_bitcast_fusion = (f32[16,1024]{1,0:T(8,128)}, f32[16,1024]{1,0:T(8,128)}) fusion(f32[2,16,1024]{2,1,0:T(8,128)S(1)} %get-tuple-element.6), kind=kLoop, calls=%fused_computation | loop fusion | flops 32768 | bytes 262144 | tf_op jit(solution)/shard_map/mul | solution.py:623
